TPU v7x, 32 devices: a whole 2x2x4 slice. The times are simulated.
32 devices in a mesh: ep: 16 (over z, y, x), tp: 2 (over core).
Axes of the slice: x: 2, y: 2, z: 4, core: 2. Of those that a mesh axis runs over, the one named last changes fastest.
Arguments:
- tokens: bfloat16 [256, 1024], P('ep'), may hold values from -6 to 6
- linear_matrix_state: float32 [256, 16, 4096], P('ep', 'tp'), may hold values from -4 to 4
- mixer_norm_gain: float32 [1024], replicated, may hold values from 0.1 to 1.9
- receptance_weight: bfloat16 [1024, 1024], P(None, 'tp'), may hold values from -0.1875 to 0.1875
- key_weight: bfloat16 [1024, 1024], P(None, 'tp'), may hold values from -0.1875 to 0.1875
- value_weight: bfloat16 [1024, 1024], P(None, 'tp'), may hold values from -0.1875 to 0.1875
- decay_weight: bfloat16 [1024, 1024], P(None, 'tp'), may hold values from -0.1875 to 0.1875
- learning_rate_weight: bfloat16 [1024, 1024], P(None, 'tp'), may hold values from -0.1875 to 0.1875
- output_gate_weight: bfloat16 [1024, 1024], P(None, 'tp'), may hold values from -0.1875 to 0.1875
- decay_offset_bias: float32 [1024], P('tp'), may hold values from -5 to 2
- present_position_factor: float32 [1024], P('tp'), may hold values from -2 to 2
- per_head_gain: float32 [1024], P('tp'), may hold values from 0.1 to 1.9
- head_mix_weight: bfloat16 [1024, 1024], P('tp'), may hold values from -0.1875 to 0.1875
- feedforward_gain: float32 [1024], replicated, may hold values from 0.1 to 1.9
- routing: int32 [256, 2], P('ep'), may hold values from 0 to 15, all different within a row; in each aligned block of 16 rows (0 to 15, 16 to 31, ...) at most 5 rows name the same one
- router_score: float32 [256, 2], P('ep'), may hold values from -6 to 6
- expert_gate_weight: bfloat16 [16, 1024, 1536], P('ep', None, 'tp'), may hold values from -0.1875 to 0.1875
- expert_up_weight: bfloat16 [16, 1024, 1536], P('ep', None, 'tp'), may hold values from -0.1875 to 0.1875
- expert_down_weight: bfloat16 [16, 1536, 1024], P('ep', 'tp'), may hold values from -0.15625 to 0.15625
Outputs:
- layer_out: bfloat16 [256, 1024], P('ep')
- new_state: float32 [256, 16, 4096], P('ep', 'tp')
Inputs may be any that keep to these rules, and one draw needn't show every extreme that they name: `routing`: each row names 2 different experts. Among the rows of one index of ep no expert is named more than 5 times, a bound that some block reaches.
All inputs are finite; a program needn't handle non-finite values.
Results may differ from a plain program's by a relative error of at most 0.013.
Values may be sent and summed in bfloat16 or wider, within the bound.
A program may use at most 64 MiB of HBM per device.

v0:
```python
import jax
import jax.numpy as jnp
from jax import lax
from jax.sharding import PartitionSpec as P

NORM_EPS = 1e-06
UNIT_EPS = 1e-05
HEAD_EPS = 0.00064


def rms_scale(values, gain):
    values = values.astype(jnp.float32)
    factor = lax.rsqrt(jnp.mean(values * values, axis=-1, keepdims=True) + NORM_EPS)
    return values * factor * gain


def project(normalized_input, weight):
    return jnp.dot(normalized_input, weight, preferred_element_type=jnp.float32)


def mixer_head_rows(
    normalized_input,
    linear_matrix_state,
    receptance_weight,
    key_weight,
    value_weight,
    decay_weight,
    learning_rate_weight,
    output_gate_weight,
    decay_offset_bias,
    present_position_factor,
    per_head_gain,
):
    batch_length = normalized_input.shape[0]
    head_count = linear_matrix_state.shape[1]
    head_width = key_weight.shape[1] // head_count
    shape = (batch_length, head_count, head_width)
    receptance = project(normalized_input, receptance_weight).reshape(shape)
    key = project(normalized_input, key_weight).reshape(shape)
    value = project(normalized_input, value_weight).reshape(shape)
    log_rate = (
        -jax.nn.softplus(-(decay_offset_bias + project(normalized_input, decay_weight))) - 0.5
    )
    decay = jnp.exp(-jnp.exp(log_rate)).reshape(shape)
    rate = jax.nn.sigmoid(project(normalized_input, learning_rate_weight)).reshape(shape)
    gating = jax.nn.sigmoid(project(normalized_input, output_gate_weight))
    unit = key * lax.rsqrt(jnp.sum(key * key, axis=-1, keepdims=True) + UNIT_EPS)
    shifted_key = key * rate
    matrix = linear_matrix_state.reshape(batch_length, head_count, head_width, head_width)
    removed = jnp.sum(matrix * unit[:, :, None, :], axis=-1)
    updated = (
        matrix * decay[:, :, None, :]
        - removed[..., None] * (unit * rate)[:, :, None, :]
        + value[..., None] * shifted_key[:, :, None, :]
    )
    read = jnp.sum(updated * receptance[:, :, None, :], axis=-1)
    center = read - jnp.mean(read, axis=-1, keepdims=True)
    scaled = center * lax.rsqrt(jnp.mean(center * center, axis=-1, keepdims=True) + HEAD_EPS)
    scaled = scaled * per_head_gain.reshape(head_count, head_width)
    own_term = (
        jnp.sum(
            receptance * shifted_key * present_position_factor.reshape(head_count, head_width),
            axis=-1,
            keepdims=True,
        )
        * value
    )
    merged = ((scaled + own_term).reshape(batch_length, head_count * head_width) * gating).astype(
        jnp.bfloat16
    )
    return (merged, updated.reshape(batch_length, head_count, head_width * head_width))


def body(
    tokens,
    linear_matrix_state,
    mixer_norm_gain,
    receptance_weight,
    key_weight,
    value_weight,
    decay_weight,
    learning_rate_weight,
    output_gate_weight,
    decay_offset_bias,
    present_position_factor,
    per_head_gain,
    head_mix_weight,
    feedforward_gain,
    routing,
    router_score,
    expert_gate_weight,
    expert_up_weight,
    expert_down_weight,
):
    seq_count, model_width = tokens.shape
    normalized_input = rms_scale(tokens, mixer_norm_gain).astype(jnp.bfloat16)
    merged, new_state = mixer_head_rows(
        normalized_input,
        linear_matrix_state,
        receptance_weight,
        key_weight,
        value_weight,
        decay_weight,
        learning_rate_weight,
        output_gate_weight,
        decay_offset_bias,
        present_position_factor,
        per_head_gain,
    )
    partial_value = jnp.dot(merged, head_mix_weight, preferred_element_type=jnp.float32)
    mix = lax.psum(partial_value.astype(jnp.bfloat16), "tp")
    residual = tokens.astype(jnp.float32) + mix.astype(jnp.float32)
    expert_in = rms_scale(residual, feedforward_gain).astype(jnp.bfloat16)
    route_count = routing.shape[1]
    experts = lax.axis_size("ep")
    capacity = max(2, 8 * seq_count * route_count // (3 * experts))
    flat_route = routing.reshape(-1)
    onehot = (flat_route[:, None] == jnp.arange(experts, dtype=jnp.int32)[None, :]).astype(
        jnp.int32
    )
    earlier = jnp.cumsum(onehot, axis=0) - onehot
    slot = jnp.sum(earlier * onehot, axis=1)
    target = flat_route * capacity + slot
    place = (target[None, :] == jnp.arange(experts * capacity, dtype=jnp.int32)[:, None]).astype(
        jnp.bfloat16
    )
    repeated = jnp.broadcast_to(expert_in[:, None, :], (seq_count, route_count, model_width))
    repeated = repeated.reshape(seq_count * route_count, model_width)
    outgoing = jnp.dot(place, repeated, preferred_element_type=jnp.float32).astype(jnp.bfloat16)
    outgoing = outgoing.reshape(experts, capacity, model_width)
    half_width = model_width // lax.axis_size("tp")
    own_half = lax.dynamic_slice_in_dim(outgoing, lax.axis_index("tp") * half_width, half_width, 2)
    whole_rows = lax.all_gather(
        lax.all_to_all(own_half, "ep", split_axis=0, concat_axis=0, tiled=True),
        "tp",
        axis=2,
        tiled=True,
    )
    flat_rows = whole_rows.reshape(-1, whole_rows.shape[-1])
    gate_in = jnp.dot(flat_rows, expert_gate_weight[0], preferred_element_type=jnp.float32)
    up_in = jnp.dot(flat_rows, expert_up_weight[0], preferred_element_type=jnp.float32)
    hidden = (jax.nn.silu(gate_in) * up_in).astype(jnp.bfloat16)
    summed = lax.psum_scatter(
        jnp.dot(hidden, expert_down_weight[0], preferred_element_type=jnp.float32)
        .reshape(whole_rows.shape)
        .astype(jnp.bfloat16),
        "tp",
        scatter_dimension=2,
        tiled=True,
    )
    returned_half = lax.all_to_all(summed, "ep", split_axis=0, concat_axis=0, tiled=True)
    returned = lax.all_gather(returned_half, "tp", axis=2, tiled=True)
    routed = jnp.einsum(
        "sj,sd->jd",
        place,
        returned.reshape(experts * capacity, model_width),
        preferred_element_type=jnp.float32,
    )
    routed = routed.reshape(seq_count, route_count, model_width)
    first = jax.nn.sigmoid(router_score[:, 0] - router_score[:, 1])
    second = jax.nn.sigmoid(router_score[:, 1] - router_score[:, 0])
    weights = jnp.stack([first, second], axis=1)
    layer_out = (residual + jnp.sum(weights[:, :, None] * routed, axis=1)).astype(jnp.bfloat16)
    return (layer_out, new_state)


def solution(mesh):
    return jax.shard_map(
        body,
        mesh=mesh,
        in_specs=(
            P("ep", None),
            P("ep", "tp", None),
            P(),
            P(None, "tp"),
            P(None, "tp"),
            P(None, "tp"),
            P(None, "tp"),
            P(None, "tp"),
            P(None, "tp"),
            P("tp"),
            P("tp"),
            P("tp"),
            P("tp", None),
            P(),
            P("ep", None),
            P("ep", None),
            P("ep", None, "tp"),
            P("ep", None, "tp"),
            P("ep", "tp", None),
        ),
        out_specs=(P("ep", None), P("ep", "tp", None)),
        check_vma=False,
    )
```

profile of v0, /device:TPU:0, one launch (start us, length us, event | category | flops | bytes accessed | tf_op | source)
XLA Modules:
  0.0 133.6 jit_solution(7547226032470158027)
XLA Ops:
  7.2 0.0 copy-start
  7.2 0.0 copy-start.1
  7.2 0.0 copy-start.4
  7.2 0.0 reduce-scatter.2.cloned.1.call-start
  7.3 1.0 fusion.33
  8.3 1.6 %fusion.62 = f32[16,512]{1,0:T(8,128)S(1)} fusion(bf16[1024,512]{1,0:T(8,128)(2,1)} %param.23, bf16[16,1024]{1,0:T(8,128)(2,1)} %param.19, f32[1024]{0:T(1024)} %param.21, f32[16]{0:T(128)S(1)} %add_rsqrt_fusion.3), kind=kOutput, calls=%fused_computation.86 | convolution fusion | flops 16842752 | bytes 1118272 | tf_op jit(solution)/shard_map/dot_general | solution.py:18
  9.9 0.1 reshape.152
  9.9 0.1 multiply_reduce_fusion.6
  10.1 1.6 %fusion.29 = f32[16,512]{1,0:T(8,128)S(1)} fusion(bf16[1024,512]{1,0:T(8,128)(2,1)} %param.26, bf16[16,1024]{1,0:T(8,128)(2,1)} %param.19, f32[1024]{0:T(1024)} %param.21, f32[16]{0:T(128)S(1)} %add_rsqrt_fusion.3), kind=kOutput, calls=%fused_computation.31 | convolution fusion | flops 16867328 | bytes 1118272 | tf_op jit(solution)/shard_map/dot_general | solution.py:18
  11.6 0.1 reshape.153
  11.7 0.0 copy-done.1
  11.7 0.3 fusion.57
  12.0 0.1 mul.256
  12.1 1.6 %fusion.41 = f32[16,512]{1,0:T(8,128)S(1)} fusion(bf16[1024,512]{1,0:T(8,128)(2,1)} %param.25, f32[512]{0:T(512)S(1)} %copy-done.7, bf16[16,1024]{1,0:T(8,128)(2,1)S(1)} %copy-done.1, f32[1024]{0:T(1024)S(1)} %copy-done.4, f32[16]{0:T(128)S(1)} %add_rsqrt_fusion.3), kind=kOutput, calls=%fused_computation.56 | convolution fusion | flops 16932864 | bytes 1120320 | tf_op jit(solution)/shard_map/dot_general | solution.py:18
  13.7 0.1 mul.239
  13.7 1.5 %fusion.59 = f32[16,512]{1,0:T(8,128)S(1)} fusion(bf16[1024,512]{1,0:T(8,128)(2,1)} %param.24, bf16[16,1024]{1,0:T(8,128)(2,1)S(1)} %copy-done.1, f32[1024]{0:T(1024)S(1)} %copy-done.4, f32[16]{0:T(128)S(1)} %add_rsqrt_fusion.3), kind=kOutput, calls=%fused_computation.85 | convolution fusion | flops 16842752 | bytes 1118272 | tf_op jit(solution)/shard_map/dot_general | solution.py:18
  15.3 0.1 mul.251
  15.3 4.6 %reshape.151 = f32[16,8,64,64]{3,2,1,0:T(8,128)} reshape(f32[16,8,4096]{2,1,0:T(8,128)} %param.20) | data formatting | bytes 4194304 | tf_op jit(solution)/shard_map/reshape | solution.py:49
  19.9 0.1 fusion.65
  20.0 20.4 %broadcast_multiply_fusion = (f32[16,8,64,64]{3,2,1,0:T(8,128)}, f32[16,8,64]{2,1,0:T(8,128)S(1)}, f32[16,8,64,64]{3,2,1,0:T(8,128)}) fusion(f32[16,8,64]{2,1,0:T(8,128)S(1)} %get-tuple-element.8, f32[16,8,64]{2,1,0:T(8,128)S(1)} %mul.251, f32[16,8,64]{2,1,0:T(8,128)S(1)} %mul.256, f32[16,8,64,64]{3,2,1,0:T(8,128)} %reshape.151, f32[16,8,64]{2,1,0:T(8,128)S(1)} %mul.239, ...), kind=kOutput, calls=%fused_computation.8 | output fusion | flops 4194367 | bytes 6520832 | tf_op jit(solution)/shard_map/mul | solution.py:53
  40.4 4.8 %mul.261 = f32[16,8,4096]{2,1,0:T(8,128)} reshape(f32[16,8,64,64]{3,2,1,0:T(8,128)} %get-tuple-element.11) | data formatting | bytes 4194304 | tf_op jit(solution)/shard_map/mul | solution.py:53
  45.2 4.8 %mul.262 = f32[16,8,4096]{2,1,0:T(8,128)} reshape(f32[16,8,64,64]{3,2,1,0:T(8,128)} %get-tuple-element.6) | data formatting | bytes 4194304 | tf_op jit(solution)/shard_map/mul | solution.py:54
  50.0 2.2 %mul.257 = f32[16,8,64,64]{3,2,1,0:T(8,128)} broadcast(f32[16,8,64]{2,1,0:T(8,128)S(1)} %mul.256), dimensions={0,1,3} | broadcast | bytes 2129920 | tf_op jit(solution)/shard_map/mul | solution.py:56
  52.1 4.8 %mul.263 = f32[16,8,4096]{2,1,0:T(8,128)} reshape(f32[16,8,64,64]{3,2,1,0:T(8,128)} %mul.257) | data formatting | bytes 4194304 | tf_op jit(solution)/shard_map/mul | solution.py:56
  56.9 2.2 %mul.240 = f32[16,8,64,64]{3,2,1,0:T(8,128)} broadcast(f32[16,8,64]{2,1,0:T(8,128)S(1)} %mul.239), dimensions={0,1,3} | broadcast | bytes 2129920 | tf_op jit(solution)/shard_map/mul | solution.py:52
  59.1 4.8 %mul.259 = f32[16,8,4096]{2,1,0:T(8,128)} reshape(f32[16,8,64,64]{3,2,1,0:T(8,128)} %mul.240) | data formatting | bytes 4194304 | tf_op jit(solution)/shard_map/mul | solution.py:52
  63.9 5.9 %multiply_reduce_fusion.2 = (f32[16,8]{1,0:T(8,128)S(1)}, f32[16,8,4096]{2,1,0:T(8,128)}) fusion(f32[16,8,4096]{2,1,0:T(8,128)} %mul.263, f32[16,8,4096]{2,1,0:T(8,128)} %mul.262, f32[16,8,4096]{2,1,0:T(8,128)} %mul.261, f32[16,8,4096]{2,1,0:T(8,128)} %param.20, f32[16,8,4096]{2,1,0:T(8,128)} %mul.259), kind=kLoop, calls=%fused_computation.6 | loop fusion | flops 2621312 | bytes 12583424 | tf_op jit(solution)/shard_map/reduce_sum | solution.py:57
  69.7 0.2 multiply_reduce_fusion.5
  69.9 0.1 subtract_multiply_fusion
  70.0 0.1 mul.268
  70.1 0.1 mul.272
  70.2 0.5 fusion
  70.7 0.1 mul.276
  70.8 0.0 copy-done.9
  70.8 2.2 %convolution_convert_fusion.1 = bf16[16,1024]{1,0:T(8,128)(2,1)S(1)} fusion(bf16[512,1024]{1,0:T(8,128)(2,1)} %param.31, bf16[1024,512]{1,0:T(8,128)(2,1)} %param.27, f32[16,512]{1,0:T(8,128)S(1)} %mul.276, f32[16,512]{1,0:T(8,128)S(1)} %fusion.59, f32[16,512]{1,0:T(8,128)S(1)} %mul.268, f32[512]{0:T(512)S(1)} %copy-done.9, ...), kind=kOutput, calls=%fused_computation.22 | convolution fusion | flops 33701888 | bytes 2267200 | tf_op jit(solution)/shard_map/dot_general | solution.py:110
  73.0 3.7 %psum.7 = bf16[16,1024]{1,0:T(8,128)(2,1)S(1)} all-reduce(bf16[16,1024]{1,0:T(8,128)(2,1)S(1)} %convolution_convert_fusion.1), channel_id=1, replica_groups=mesh['ep'=16,'tp'=2] {'tp'}, use_global_device_ids=true, to_apply=%region_7.8 | all-reduce | flops 16384 | bytes 65536 | tf_op jit(solution)/shard_map/psum | solution.py:111
  76.7 0.1 multiply_reduce_fusion.3
  76.8 0.1 multiply_convert_fusion
  77.0 0.1 copy.38
  77.1 0.1 reshape.154
  77.2 0.1 fusion.48
  77.3 0.1 reduce_window_sum.11
  77.3 0.2 select_reduce_fusion
  77.5 0.2 convolution_convert_fusion
  77.7 0.8 reshape.156
  78.5 0.9 constant_dynamic-slice_fusion
  79.4 15.8 %all_to_all.10 = bf16[16,5,512]{2,1,0:T(8,128)(2,1)S(1)} all-to-all(bf16[16,5,512]{2,1,0:T(8,128)(2,1)S(1)} %constant_dynamic-slice_fusion), channel_id=1, replica_groups=mesh['ep'=16,'tp'=2] {'ep'}, dimensions={0} | all-to-all | bytes 163840 | tf_op jit(solution)/shard_map/all_to_all | solution.py:134
  95.1 2.0 %all_gather.6 = bf16[16,5,1024]{2,1,0:T(8,128)(2,1)S(1)} all-gather(bf16[16,5,512]{2,1,0:T(8,128)(2,1)S(1)} %all_to_all.10), channel_id=1, replica_groups=mesh['ep'=16,'tp'=2] {'tp'}, dimensions={2}, use_global_device_ids=true | all-gather | bytes 245760 | tf_op jit(solution)/shard_map/all_gather | solution.py:133
  97.1 0.7 reshape.157
  97.8 1.3 fusion.11
  99.2 1.9 %fusion.19 = bf16[80,768]{1,0:T(8,128)(2,1)S(1)} fusion(bf16[80,1024]{1,0:T(8,128)(2,1)} %reshape.157, bf16[1,1024,768]{2,1,0:T(8,128)(2,1)} %param.36, f32[80,768]{1,0:T(8,128)S(1)} %fusion.11), kind=kOutput, calls=%fused_computation.19 | convolution fusion | flops 126197760 | bytes 2105344 | tf_op jit(solution)/shard_map/dot_general | solution.py:141
  101.1 0.1 dot_general.48
  101.2 1.1 fusion.16
  102.2 0.0 reduce-scatter.2.cloned.1.call-update
  102.2 0.1 reduce_sum.100
  102.3 0.1 copy.39
  102.4 5.2 %reduce-scatter.2.cloned.1.call-done = bf16[16,5,512]{2,0,1:T(8,128)(2,1)} async-done(((bf16[16,5,1024]{2,0,1:T(8,128)(2,1)}), bf16[16,5,512]{2,0,1:T(8,128)(2,1)}) %reduce-scatter.2.cloned.1.call-update) | async-done | bytes 81936 | tf_op jit(solution)/shard_map/reduce_scatter | solution.py:143
  107.6 1.6 %copy.41 = bf16[16,5,512]{2,1,0:T(8,128)(2,1)} copy(bf16[16,5,512]{2,0,1:T(8,128)(2,1)} %reduce-scatter.2.cloned.1.call-done) | data formatting | bytes 163840 | tf_op jit(solution)/shard_map/reduce_scatter | solution.py:143
  109.1 6.7 %all-to-all-start.1 = ((bf16[16,5,512]{2,1,0:T(8,128)(2,1)}), bf16[16,5,512]{2,1,0:T(8,128)(2,1)S(1)}, u32[]{:S(2)}, u32[]{:S(2)}) async-start(bf16[16,5,512]{2,1,0:T(8,128)(2,1)} %copy.41), calls=%async_computation.2 | async-start | bytes 262144 | tf_op jit(solution)/shard_map/all_to_all | solution.py:151
  115.9 7.9 %all-to-all-done.1 = bf16[16,5,512]{2,1,0:T(8,128)(2,1)S(1)} async-done(((bf16[16,5,512]{2,1,0:T(8,128)(2,1)}), bf16[16,5,512]{2,1,0:T(8,128)(2,1)S(1)}, u32[]{:S(2)}, u32[]{:S(2)}) %all-to-all-start.1) | async-done | bytes 81952 | tf_op jit(solution)/shard_map/all_to_all | solution.py:151
  123.8 2.0 %all_gather.7 = bf16[16,5,1024]{2,1,0:T(8,128)(2,1)S(1)} all-gather(bf16[16,5,512]{2,1,0:T(8,128)(2,1)S(1)} %all-to-all-done.1), channel_id=1, replica_groups=mesh['ep'=16,'tp'=2] {'tp'}, dimensions={2}, use_global_device_ids=true | all-gather | bytes 245760 | tf_op jit(solution)/shard_map/all_gather | solution.py:152
  125.8 0.1 reshape.160
  125.9 0.2 fusion.22
  126.1 0.6 add_convert_fusion
  (28 shorter events, 0.2 us)
Async XLA Ops:
  7.2 94.0 %copy-start = (bf16[1,768,1024]{2,1,0:T(8,128)(2,1)S(1)}, bf16[1,768,1024]{2,1,0:T(8,128)(2,1)}, u32[]{:S(2)}) copy-start(bf16[1,768,1024]{2,1,0:T(8,128)(2,1)} %param.37) | copy-start | bytes 4718596
  7.2 4.5 %copy-start.1 = (bf16[16,1024]{1,0:T(8,128)(2,1)S(1)}, bf16[16,1024]{1,0:T(8,128)(2,1)}, u32[]{:S(2)}) copy-start(bf16[16,1024]{1,0:T(8,128)(2,1)} %param.19) | copy-start | bytes 98308
  7.2 4.5 %copy-start.4 = (f32[1024]{0:T(1024)S(1)}, f32[1024]{0:T(1024)}, u32[]{:S(2)}) copy-start(f32[1024]{0:T(1024)} %param.21) | copy-start | bytes 12292
  7.2 4.5 %copy-start.3 = (bf16[1024,512]{1,0:T(8,128)(2,1)S(1)}, bf16[1024,512]{1,0:T(8,128)(2,1)}, u32[]{:S(2)}) copy-start(bf16[1024,512]{1,0:T(8,128)(2,1)} %param.22) | copy-start | bytes 3145732
  7.2 4.9 %copy-start.7 = (f32[512]{0:T(512)S(1)}, f32[512]{0:T(512)}, u32[]{:S(2)}) copy-start(f32[512]{0:T(512)} %param.28) | copy-start | bytes 6148
  7.2 100.3 %reduce-scatter.2.cloned.1.call-start = ((), (), s32[]{:S(2)}) async-start(), calls=%async_computation.3 | async-start | bytes 245760 | tf_op jit(solution)/shard_map/reduce_scatter | solution.py:143
  63.9 6.2 %copy-start.8 = (f32[512]{0:T(512)S(1)}, f32[512]{0:T(512)}, u32[]{:S(2)}) copy-start(f32[512]{0:T(512)} %param.29) | copy-start | bytes 6148
  63.9 6.9 %copy-start.9 = (f32[512]{0:T(512)S(1)}, f32[512]{0:T(512)}, u32[]{:S(2)}) copy-start(f32[512]{0:T(512)} %param.30) | copy-start | bytes 6148
  69.7 7.1 %copy-start.5 = (f32[1024]{0:T(1024)S(1)}, f32[1024]{0:T(1024)}, u32[]{:S(2)}) copy-start(f32[1024]{0:T(1024)} %param.32) | copy-start | bytes 12292
  69.7 7.3 %copy-start.6 = (s32[16,2]{0,1:T(2,128)S(1)}, s32[16,2]{0,1:T(2,128)}, u32[]{:S(2)}) copy-start(s32[16,2]{0,1:T(2,128)} %param.33) | copy-start | bytes 388
  70.8 27.1 %copy-start.2 = (bf16[1,1024,768]{2,1,0:T(8,128)(2,1)S(1)}, bf16[1,1024,768]{2,1,0:T(8,128)(2,1)}, u32[]{:S(2)}) copy-start(bf16[1,1024,768]{2,1,0:T(8,128)(2,1)} %param.35) | copy-start | bytes 4718596
  99.1 16.7 %copy-start.10 = (f32[16,2]{0,1:T(2,128)S(1)}, f32[16,2]{0,1:T(2,128)}, u32[]{:S(2)}) copy-start(f32[16,2]{0,1:T(2,128)} %param.34) | copy-start | bytes 388
  109.1 14.7 %all-to-all-start.1 = ((bf16[16,5,512]{2,1,0:T(8,128)(2,1)}), bf16[16,5,512]{2,1,0:T(8,128)(2,1)S(1)}, u32[]{:S(2)}, u32[]{:S(2)}) async-start(bf16[16,5,512]{2,1,0:T(8,128)(2,1)} %copy.41), calls=%async_computation.2 | async-start | bytes 262144 | tf_op jit(solution)/shard_map/all_to_all | solution.py:151
Sparse Core Ops, SparseCore 0:
  102.4 5.1 reduce-scatter.1
where the time goes:
time: 134 us
  local copies, waits for them, and re-layouts  33.2 us (25%)
  other arithmetic  29.4 us (22%)
  blocking collectives  23.4 us (17%)
  between operations  14.3 us (11%)
  matrix products  13.3 us (10%)
  waiting for transfers between devices  13.1 us (10%)
  starting transfers between devices  6.76 us (5%)
    mul x1, other arithmetic, mixer_head_rows(): removed[..., None] * (unit * rate)[:, :, None, :]  20.4 us
    all_to_all x1, blocking collectives, body(): lax.all_to_all(own_half, 'ep', split_axis=0, concat_axis=0, tiled=True)  15.8 us
    all_to_all x1, waiting for transfers between devices, body(): lax.all_to_all(summed, 'ep', split_axis=0, concat_axis=0, tiled=True)  7.92 us
    mul x3, local copies, waits for them, and re-layouts, mixer_head_rows(): matrix * decay[:, :, None, :]  7.05 us
    mul x3, local copies, waits for them, and re-layouts, mixer_head_rows(): read = jnp.sum(updated * receptance[:, :, None, :], axis=-1)  7.03 us
    all_to_all x1, starting transfers between devices, body(): lax.all_to_all(summed, 'ep', split_axis=0, concat_axis=0, tiled=True)  6.72 us
    dot_general x5, matrix products, project(): return jnp.dot(normalized_input, weight, preferred_element_type=jnp.float32)  6.47 us
    reduce_sum x1, other arithmetic, mixer_head_rows(): center = read - jnp.mean(read, axis=-1, keepdims=True)  5.86 us
  transfers between devices with their start and end apart: 2, of which 2 were waited for; matrix products, arithmetic and copies ran while one was open for 0% of the time, Pallas kernels for 0%

commit v1 on v0

v1 whole, which is shorter than its diff:
```python
import functools
import math

import jax
import jax.numpy as jnp
from jax import lax
from jax.experimental import pallas as pl
from jax.experimental.pallas import tpu as pltpu
from jax.sharding import PartitionSpec as P

NORM_EPS = 1e-06
UNIT_EPS = 1e-05
HEAD_EPS = 0.00064
LANES = 128
F32 = jnp.float32
BF16 = jnp.bfloat16
HBM = pl.BlockSpec(memory_space=pl.ANY)
VMEM = pl.BlockSpec(memory_space=pltpu.VMEM)
MESH = pl.DeviceIdType.MESH
DECAY_SCALE = math.exp(-0.5)


def dot(a, b):
    return jnp.dot(a, b, preferred_element_type=F32)


def rms_scale(values, gain):
    factor = lax.rsqrt(jnp.mean(values * values, axis=-1, keepdims=True) + NORM_EPS)
    return values * factor * gain


def split(x):
    high = x.astype(BF16)
    return high, (x - high.astype(F32)).astype(BF16)


def to_head_rows(x, ref, heads):
    seqs = x.shape[0]
    low = lax.broadcasted_iota(jnp.int32, (seqs, LANES), 1) < LANES // 2
    for pair in range(heads // 2):
        here = x[:, pair * LANES : (pair + 1) * LANES]
        turned = pltpu.roll(here, LANES // 2, 1)
        ref[pl.ds(2 * pair, seqs, stride=heads), :] = jnp.where(low, here, turned)
        ref[pl.ds(2 * pair + 1, seqs, stride=heads), :] = jnp.where(low, turned, here)


def from_head_rows(ref, seqs, heads):
    low = lax.broadcasted_iota(jnp.int32, (seqs, LANES), 1) < LANES // 2
    parts = []
    for pair in range(heads // 2):
        even = ref[pl.ds(2 * pair, seqs, stride=heads), :]
        odd = ref[pl.ds(2 * pair + 1, seqs, stride=heads), :]
        parts.append(jnp.where(low, even, odd))
    return jnp.concatenate(parts, axis=1)


def mixer_kernel(
    tokens_ref,
    state_hbm,
    norm_gain_ref,
    wr_hbm,
    wk_hbm,
    wv_hbm,
    wd_hbm,
    wl_hbm,
    wg_hbm,
    bias_ref,
    factor_ref,
    head_gain_ref,
    wm_hbm,
    partial_ref,
    new_hbm,
    state,
    wr,
    wk,
    wv,
    wd,
    wl,
    wg,
    wm,
    r_rows,
    k_rows,
    v_rows,
    d_rows,
    l_rows,
    f_rows,
    g_rows,
    o_rows,
    products,
    gatherer,
    sems,
    out_sems,
):
    seqs, heads, cells = state.shape
    rows = seqs * heads
    width = LANES // 2
    sources = [wk_hbm, wr_hbm, wd_hbm, wl_hbm, state_hbm, wv_hbm, wg_hbm, wm_hbm]
    targets = [wk, wr, wd, wl, state, wv, wg, wm]
    copies = [
        pltpu.make_async_copy(a, b, sems.at[i]) for i, (a, b) in enumerate(zip(sources, targets))
    ]
    for copy in copies:
        copy.start()

    normed = rms_scale(tokens_ref[...].astype(F32), norm_gain_ref[...]).astype(BF16)
    channels = heads * width
    to_head_rows(jnp.broadcast_to(factor_ref[...], (seqs, channels)), f_rows, heads)
    to_head_rows(jnp.broadcast_to(head_gain_ref[...], (seqs, channels)), g_rows, heads)
    chunk = 512
    for c in range(cells // chunk):
        at = lax.broadcasted_iota(jnp.int32, (chunk, LANES), 0) // width
        to = lax.broadcasted_iota(jnp.int32, (chunk, LANES), 1) % width
        gatherer[pl.ds(c * chunk, chunk), :] = jnp.where(
            to - at == c * (chunk // width), 1.0, 0.0
        ).astype(BF16)

    copies[0].wait()
    to_head_rows(dot(normed, wk[...]), k_rows, heads)
    copies[1].wait()
    to_head_rows(dot(normed, wr[...]), r_rows, heads)
    copies[2].wait()
    decay_in = dot(normed, wd[...]) + bias_ref[...]
    to_head_rows(jnp.exp(-DECAY_SCALE * jax.nn.sigmoid(decay_in)), d_rows, heads)
    copies[3].wait()
    to_head_rows(jax.nn.sigmoid(dot(normed, wl[...])), l_rows, heads)

    key = k_rows[...]
    unit = key * lax.rsqrt(jnp.sum(key * key, axis=-1, keepdims=True) * 0.5 + UNIT_EPS)
    decay = d_rows[...]
    rate = l_rows[...]
    receptance = r_rows[...]
    shifted = key * rate
    unit_rate = unit * rate
    decay_receptance = decay * receptance

    copies[4].wait()
    for c in range(cells // LANES):
        lanes = pl.ds(c * LANES, LANES)
        x = state[:, :, lanes].reshape(rows, LANES)
        products[0:rows, lanes] = (x * unit).astype(BF16)
        high, low = split(x * decay_receptance)
        products[rows : 2 * rows, lanes] = high
        products[2 * rows : 3 * rows, lanes] = low
    copies[5].wait()
    to_head_rows(dot(normed, wv[...]), v_rows, heads)
    value = v_rows[...]
    sums = dot(products[...], gatherer[...])
    removed = sums[0:rows]
    read = sums[rows : 2 * rows] + sums[2 * rows :]

    def head_sum(x):
        return jnp.sum(x, axis=-1, keepdims=True) * 0.5

    read = read - removed * head_sum(unit_rate * receptance) + value * head_sum(shifted * receptance)
    center = read - head_sum(read) * (1.0 / width)
    scaled = center * lax.rsqrt(head_sum(center * center) * (1.0 / width) + HEAD_EPS)
    own = head_sum(receptance * shifted * f_rows[...])
    o_rows[...] = scaled * g_rows[...] + own * value
    copies[6].wait()
    gating = jax.nn.sigmoid(dot(normed, wg[...]))
    merged = (from_head_rows(o_rows, seqs, heads) * gating).astype(BF16)
    copies[7].wait()
    partial_ref[...] = dot(merged, wm[...]).astype(BF16)

    first = lax.broadcasted_iota(jnp.int32, (rows, LANES), 1) < width
    v_high, v_low = split(value)
    m_high, m_low = split(removed)
    compact = jnp.concatenate(
        [
            jnp.where(first, v_high.astype(F32), v_low.astype(F32)).astype(BF16),
            jnp.where(first, m_high.astype(F32), m_low.astype(F32)).astype(BF16),
        ],
        axis=0,
    )
    writes = []
    for c in range(cells // chunk):
        spread = lax.dot_general(
            compact,
            gatherer[pl.ds(c * chunk, chunk), :],
            (((1,), (1,)), ((), ())),
            preferred_element_type=F32,
        )
        for b in range(chunk // LANES):
            lanes = pl.ds(c * chunk + b * LANES, LANES)
            x = state[:, :, lanes].reshape(rows, LANES)
            v_here = spread[0:rows, b * LANES : (b + 1) * LANES]
            m_here = spread[rows:, b * LANES : (b + 1) * LANES]
            new = x * decay + v_here * shifted - m_here * unit_rate
            state[:, :, lanes] = new.reshape(seqs, heads, LANES)
        part = pl.ds(c * chunk, chunk)
        write = pltpu.make_async_copy(
            state.at[:, :, part], new_hbm.at[:, :, part], out_sems.at[c]
        )
        write.start()
        writes.append(write)
    for write in writes:
        write.wait()


def expert_kernel(
    experts,
    capacity,
    tokens_ref,
    partial_ref,
    gain_ref,
    routing_ref,
    score_ref,
    gate_hbm,
    up_hbm,
    down_hbm,
    out_ref,
    wg,
    wu,
    wd,
    other_partial,
    features,
    outgoing,
    arrived,
    paired,
    crossing,
    crossed,
    results,
    returned,
    final,
    w_sems,
    pair_send,
    pair_recv,
    go_send,
    go_recv,
    fwd_send,
    fwd_recv,
    back_send,
    back_recv,
    local_sems,
):
    me = lax.axis_index("ep")
    side = lax.axis_index("tp")
    other = 1 - side
    seqs, model = tokens_ref.shape
    half = model // 2
    rows = experts * capacity

    barrier = pltpu.get_barrier_semaphore()
    pl.semaphore_signal(barrier, inc=1, device_id=(me, other), device_id_type=MESH)

    @pl.loop(1, experts)
    def _(k):
        pl.semaphore_signal(
            barrier, inc=1, device_id=(lax.rem(me + k, experts), side), device_id_type=MESH
        )

    loads = [
        pltpu.make_async_copy(a.at[0], b, w_sems.at[i])
        for i, (a, b) in enumerate([(gate_hbm, wg), (up_hbm, wu), (down_hbm, wd)])
    ]
    for load in loads:
        load.start()

    route0 = routing_ref[:, 0:1]
    route1 = routing_ref[:, 1:2]
    names = lax.broadcasted_iota(jnp.int32, (seqs, experts), 1)
    hot0 = jnp.where(route0 == names, 1.0, 0.0)
    hot1 = jnp.where(route1 == names, 1.0, 0.0)
    below = jnp.where(
        lax.broadcasted_iota(jnp.int32, (seqs, seqs), 1)
        < lax.broadcasted_iota(jnp.int32, (seqs, seqs), 0),
        1.0,
        0.0,
    ).astype(BF16)
    before0 = dot(below, hot0.astype(BF16))
    before1 = dot(below, hot1.astype(BF16)) + jnp.sum(hot0, axis=0, keepdims=True)
    slot0 = jnp.sum(before0 * hot0, axis=1, keepdims=True).astype(jnp.int32)
    slot1 = jnp.sum(before1 * hot1, axis=1, keepdims=True).astype(jnp.int32)
    spots = lax.broadcasted_iota(jnp.int32, (seqs, rows), 1)
    place0 = jnp.where(route0 * capacity + slot0 == spots, 1.0, 0.0)
    place1 = jnp.where(route1 * capacity + slot1 == spots, 1.0, 0.0)
    placed = (place0 + place1).astype(BF16)
    place0 = place0.astype(BF16)
    place1 = place1.astype(BF16)
    difference = score_ref[:, 0:1] - score_ref[:, 1:2]
    weight0 = jax.nn.sigmoid(difference)
    weight1 = jax.nn.sigmoid(-difference)

    pl.semaphore_wait(barrier, experts)

    def to_pair(source, target, index):
        return pltpu.make_async_remote_copy(
            src_ref=source,
            dst_ref=target,
            send_sem=pair_send.at[index],
            recv_sem=pair_recv.at[index],
            device_id=(me, other),
            device_id_type=MESH,
        )

    mix_copy = to_pair(partial_ref, other_partial, 0)
    mix_copy.start()
    mix_copy.wait()
    mix = (partial_ref[...].astype(F32) + other_partial[...].astype(F32)).astype(BF16)
    residual = tokens_ref[...].astype(F32) + mix.astype(F32)
    expert_in = rms_scale(residual, gain_ref[...])
    own_lanes = pl.ds(pl.multiple_of(side * half, LANES), half)
    other_lanes = pl.ds(pl.multiple_of(other * half, LANES), half)
    mine = jnp.where(side == 0, expert_in[:, :half], expert_in[:, half:]).astype(BF16)
    own_residual = jnp.where(side == 0, residual[:, :half], residual[:, half:])
    packed = lax.dot_general(
        placed, mine, (((0,), (0,)), ((), ())), preferred_element_type=F32
    )
    outgoing[...] = packed.reshape(experts, capacity, half).astype(BF16)

    def go(k):
        peer = lax.rem(me + k, experts)
        return pltpu.make_async_remote_copy(
            src_ref=outgoing.at[peer],
            dst_ref=arrived.at[me],
            send_sem=go_send.at[k],
            recv_sem=go_recv.at[k],
            device_id=(peer, side),
            device_id_type=MESH,
        )

    def forward(k):
        source = lax.rem(me - k + experts, experts)
        return pltpu.make_async_remote_copy(
            src_ref=arrived.at[source],
            dst_ref=paired.at[source],
            send_sem=fwd_send.at[k],
            recv_sem=fwd_recv.at[k],
            device_id=(me, other),
            device_id_type=MESH,
        )

    @pl.loop(1, experts)
    def _(k):
        go(k).start()

    keep = pltpu.make_async_copy(outgoing.at[me], arrived.at[me], local_sems.at[0])
    keep.start()
    keep.wait()
    forward(0).start()

    @pl.loop(1, experts)
    def _(k):
        go(k).wait_recv()
        forward(k).start()

    own_rows = pl.ds(pl.multiple_of(side * half, LANES), half)
    other_rows = pl.ds(pl.multiple_of(other * half, LANES), half)
    x = arrived[...].astype(F32).reshape(rows, half).astype(BF16)
    loads[0].wait()
    loads[1].wait()
    gate = dot(x, wg[own_rows, :])
    up = dot(x, wu[own_rows, :])

    @pl.loop(0, experts)
    def _(k):
        forward(k).wait_recv()

    x = paired[...].astype(F32).reshape(rows, half).astype(BF16)
    gate = gate + dot(x, wg[other_rows, :])
    up = up + dot(x, wu[other_rows, :])
    hidden = (jax.nn.silu(gate) * up).astype(BF16)
    loads[2].wait()
    crossing[...] = dot(hidden, wd[:, other_lanes]).astype(BF16)
    cross_copy = to_pair(crossing, crossed, 1)
    cross_copy.start()
    own_result = dot(hidden, wd[:, own_lanes])
    cross_copy.wait()
    own_result = own_result + crossed[...].astype(F32)
    results[...] = own_result.reshape(experts, capacity, half).astype(BF16)

    def back(k):
        peer = lax.rem(me + k, experts)
        return pltpu.make_async_remote_copy(
            src_ref=results.at[peer],
            dst_ref=returned.at[me],
            send_sem=back_send.at[k],
            recv_sem=back_recv.at[k],
            device_id=(peer, side),
            device_id_type=MESH,
        )

    @pl.loop(1, experts)
    def _(k):
        back(k).start()

    keep = pltpu.make_async_copy(results.at[me], returned.at[me], local_sems.at[1])
    keep.start()
    keep.wait()

    @pl.loop(1, experts)
    def _(k):
        back(k).wait_recv()

    y = returned[...].astype(F32).reshape(rows, half).astype(BF16)
    final[...] = (own_residual + weight0 * dot(place0, y) + weight1 * dot(place1, y)).astype(BF16)
    final_copy = to_pair(final, out_ref.at[:, own_lanes], 2)
    final_copy.start()
    out_ref[:, own_lanes] = final[...]
    final_copy.wait()

    forward(0).wait_send()

    @pl.loop(1, experts)
    def _(k):
        go(k).wait_send()
        forward(k).wait_send()
        back(k).wait_send()


def body(
    tokens,
    linear_matrix_state,
    mixer_norm_gain,
    receptance_weight,
    key_weight,
    value_weight,
    decay_weight,
    learning_rate_weight,
    output_gate_weight,
    decay_offset_bias,
    present_position_factor,
    per_head_gain,
    head_mix_weight,
    feedforward_gain,
    routing,
    router_score,
    expert_gate_weight,
    expert_up_weight,
    expert_down_weight,
):
    seqs, model = tokens.shape
    _, heads, cells = linear_matrix_state.shape
    rows = seqs * heads
    weights = (
        receptance_weight,
        key_weight,
        value_weight,
        decay_weight,
        learning_rate_weight,
        output_gate_weight,
    )
    head_rows = pltpu.VMEM((rows, LANES), F32)
    partial, new_state = pl.pallas_call(
        mixer_kernel,
        out_shape=(
            jax.ShapeDtypeStruct((seqs, model), BF16),
            jax.ShapeDtypeStruct(linear_matrix_state.shape, F32),
        ),
        in_specs=[VMEM, HBM, VMEM] + [HBM] * 6 + [VMEM] * 3 + [HBM],
        out_specs=(VMEM, HBM),
        scratch_shapes=[pltpu.VMEM(linear_matrix_state.shape, F32)]
        + [pltpu.VMEM(w.shape, BF16) for w in weights]
        + [pltpu.VMEM(head_mix_weight.shape, BF16)]
        + [head_rows] * 8
        + [
            pltpu.VMEM((3 * rows, cells), BF16),
            pltpu.VMEM((cells, LANES), BF16),
            pltpu.SemaphoreType.DMA((8,)),
            pltpu.SemaphoreType.DMA((cells // 512,)),
        ],
        name="mixer",
    )(
        tokens,
        linear_matrix_state,
        mixer_norm_gain.reshape(1, -1),
        *weights,
        decay_offset_bias.reshape(1, -1),
        present_position_factor.reshape(1, -1),
        per_head_gain.reshape(1, -1),
        head_mix_weight,
    )

    experts = lax.axis_size("ep")
    capacity = max(2, 8 * seqs * routing.shape[1] // (3 * experts))
    capacity = -(-capacity // 8) * 8
    half = model // 2
    exchange = pltpu.VMEM((experts, capacity, half), BF16)
    layer_out = pl.pallas_call(
        functools.partial(expert_kernel, experts, capacity),
        out_shape=jax.ShapeDtypeStruct((seqs, model), BF16),
        in_specs=[VMEM] * 5 + [HBM] * 3,
        out_specs=VMEM,
        scratch_shapes=[
            pltpu.VMEM(expert_gate_weight.shape[1:], BF16),
            pltpu.VMEM(expert_up_weight.shape[1:], BF16),
            pltpu.VMEM(expert_down_weight.shape[1:], BF16),
            pltpu.VMEM((seqs, model), BF16),
            pltpu.VMEM((seqs, model), BF16),
            exchange,
            exchange,
            exchange,
            pltpu.VMEM((experts * capacity, half), BF16),
            pltpu.VMEM((experts * capacity, half), BF16),
            exchange,
            exchange,
            pltpu.VMEM((seqs, half), BF16),
            pltpu.SemaphoreType.DMA((3,)),
            pltpu.SemaphoreType.DMA((3,)),
            pltpu.SemaphoreType.DMA((3,)),
        ]
        + [pltpu.SemaphoreType.DMA((experts,))] * 6
        + [pltpu.SemaphoreType.DMA((2,))],
        compiler_params=pltpu.CompilerParams(collective_id=0, has_side_effects=True),
        name="experts",
    )(
        tokens,
        partial,
        feedforward_gain.reshape(1, -1),
        routing,
        router_score,
        expert_gate_weight,
        expert_up_weight,
        expert_down_weight,
    )
    return (layer_out, new_state)


def solution(mesh):
    return jax.shard_map(
        body,
        mesh=mesh,
        in_specs=(
            P("ep", None),
            P("ep", "tp", None),
            P(),
            P(None, "tp"),
            P(None, "tp"),
            P(None, "tp"),
            P(None, "tp"),
            P(None, "tp"),
            P(None, "tp"),
            P("tp"),
            P("tp"),
            P("tp"),
            P("tp", None),
            P(),
            P("ep", None),
            P("ep", None),
            P("ep", None, "tp"),
            P("ep", None, "tp"),
            P("ep", "tp", None),
        ),
        out_specs=(P("ep", None), P("ep", "tp", None)),
        check_vma=False,
    )
```

time: 134 us -> 40.6 us (0.30)
  Pallas kernels: 0 us -> 35.5 us
  other arithmetic: 29.4 us -> 0 us
  local copies, waits for them, and re-layouts: 33.2 us -> 4.07 us
  blocking collectives: 23.4 us -> 0 us
  between operations: 14.3 us -> 0.65 us
  matrix products: 13.3 us -> 0 us
  waiting for transfers between devices: 13.1 us -> 0 us
  starting transfers between devices: 6.76 us -> 0 us
    pallas_call x0 -> x2, Pallas kernels: none -> 35.5 us  [the longest x1 25.6 us: body(): pl.pallas_call(functools.partial(expert_kernel, experts, capacity), out_s...]
    mul x12 -> x0, local copies, waits for them, and re-layouts: 23.9 us -> none  [the longest x3 7.05 us: mixer_head_rows(): matrix * decay[:, :, None, :]]
    mul x4 -> x0, other arithmetic: 21.1 us -> none  [the longest x1 20.4 us: mixer_head_rows(): removed[..., None] * (unit * rate)[:, :, None, :]]
    all_to_all x1 -> x0, blocking collectives: 15.8 us -> none  [body(): lax.all_to_all(own_half, 'ep', split_axis=0, concat_axis=0, tiled=True)]
    dot_general x11 -> x0, matrix products: 13.3 us -> none  [the longest x5 6.47 us: project(): return jnp.dot(normalized_input, weight, preferred_element_type=jnp.float32)]
    all_to_all x1 -> x0, waiting for transfers between devices: 7.92 us -> none  [body(): lax.all_to_all(summed, 'ep', split_axis=0, concat_axis=0, tiled=True)]
    reduce_sum x6 -> x0, other arithmetic: 7.45 us -> none  [the longest x1 5.86 us: mixer_head_rows(): center = read - jnp.mean(read, axis=-1, keepdims=True)]
    all_to_all x1 -> x0, starting transfers between devices: 6.72 us -> none  [body(): lax.all_to_all(summed, 'ep', split_axis=0, concat_axis=0, tiled=True)]
  transfers between devices with their start and end apart: 2 -> 0, of which waited for: 2 -> 0; matrix products, arithmetic and copies ran while one was open for 0% -> 0% of each run, Pallas kernels for 0% -> 0%
where the time goes in v1:
time: 40.6 us; the launch traced here: 40.3 us
  Pallas kernels  35.5 us (87%)
  local copies, waits for them, and re-layouts  4.07 us (10%)
  between operations  0.65 us (2%)
    pallas_call x1, Pallas kernels, body(): pl.pallas_call(functools.partial(expert_kernel, experts, capacity), out_s...  25.6 us
    pallas_call x1, Pallas kernels, body(): pl.pallas_call(mixer_kernel, out_shape=(jax.ShapeDtypeStruct((seqs, model...  9.98 us
    unnamed x3, local copies, waits for them, and re-layouts  4.07 us

profile of v1, /device:TPU:0, one launch (start us, length us, event | category | flops | bytes accessed | tf_op | source)
XLA Modules:
  0.0 40.3 jit_solution(16799674065447651041)
XLA Ops:
  0.6 1.4 %copy.21.routing_ref = s32[16,2]{1,0:T(8,128)} copy(s32[16,2]{0,1:T(2,128)} %param.33) | data formatting | bytes 256 | tf_op args[14]
  2.0 1.3 %copy.22.score_ref = f32[16,2]{1,0:T(8,128)} copy(f32[16,2]{0,1:T(2,128)} %param.34) | data formatting | bytes 256 | tf_op args[15]
  3.3 10.0 %mixer.1 = (bf16[16,1024]{1,0:T(8,128)(2,1)}, f32[16,8,4096]{2,1,0:T(8,128)}) custom-call(bf16[16,1024]{1,0:T(8,128)(2,1)} %tokens_ref.3, f32[16,8,4096]{2,1,0:T(8,128)} %state_hbm.1, f32[1,1024]{1,0:T(1,128)} %bitcast.5, bf16[1024,512]{1,0:T(8,128)(2,1)} %wr_hbm.1, bf16[1024,512]{1,0:T(8,128)(2,1)} %wk_hbm.1, bf16[1024,512]{1,0:T(8,128)(2,1)} %wv_hbm.1, ...), custom_call_target="tpu_custom_call" | custom-call | tf_op jit(solution)/shard_map/mixer/pallas_call | solution.py:444
  13.3 25.6 %experts.1 = bf16[16,1024]{1,0:T(8,128)(2,1)} custom-call(bf16[16,1024]{1,0:T(8,128)(2,1)} %tokens_ref.3, bf16[16,1024]{1,0:T(8,128)(2,1)} %get-tuple-element.4.partial_ref, f32[1,1024]{1,0:T(1,128)} %bitcast.6, s32[16,2]{1,0:T(8,128)} %copy.21.routing_ref, f32[16,2]{1,0:T(8,128)} %copy.22.score_ref, bf16[1,1024,768]{2,1,0:T(8,128)(2,1)} %gate_hbm.1, ...), custom_call_target="tpu_custom_call" | custom-call | tf_op jit(solution)/shard_map/experts/pallas_call | solution.py:479
  38.9 1.4 %copy.24 = bf16[16,1024]{1,0:T(8,128)(2,1)} copy(bf16[16,1024]{1,0:T(8,128)(2,1)} %experts.1) | data formatting | bytes 65536

commit v2 on v1

v2 whole, which is shorter than its diff:
```python
import functools
import math

import jax
import jax.numpy as jnp
from jax import lax
from jax.experimental import pallas as pl
from jax.experimental.pallas import tpu as pltpu
from jax.sharding import PartitionSpec as P

NORM_EPS = 1e-06
UNIT_EPS = 1e-05
HEAD_EPS = 0.00064
LANES = 128
F32 = jnp.float32
BF16 = jnp.bfloat16
HBM = pl.BlockSpec(memory_space=pl.ANY)
VMEM = pl.BlockSpec(memory_space=pltpu.VMEM)
MESH = pl.DeviceIdType.MESH
DECAY_SCALE = math.exp(-0.5)


def dot(a, b):
    return jnp.dot(a, b, preferred_element_type=F32)


def rms_scale(values, gain):
    factor = lax.rsqrt(jnp.mean(values * values, axis=-1, keepdims=True) + NORM_EPS)
    return values * factor * gain


def split(x):
    high = x.astype(BF16)
    return high, (x - high.astype(F32)).astype(BF16)


def to_head_rows(x, ref, heads):
    seqs = x.shape[0]
    low = lax.broadcasted_iota(jnp.int32, (seqs, LANES), 1) < LANES // 2
    for pair in range(heads // 2):
        here = x[:, pair * LANES : (pair + 1) * LANES]
        turned = pltpu.roll(here, LANES // 2, 1)
        ref[pl.ds(2 * pair, seqs, stride=heads), :] = jnp.where(low, here, turned)
        ref[pl.ds(2 * pair + 1, seqs, stride=heads), :] = jnp.where(low, turned, here)


def from_head_rows(ref, seqs, heads):
    low = lax.broadcasted_iota(jnp.int32, (seqs, LANES), 1) < LANES // 2
    parts = []
    for pair in range(heads // 2):
        even = ref[pl.ds(2 * pair, seqs, stride=heads), :]
        odd = ref[pl.ds(2 * pair + 1, seqs, stride=heads), :]
        parts.append(jnp.where(low, even, odd))
    return jnp.concatenate(parts, axis=1)


def layer_kernel(
    experts,
    capacity,
    sent,
    tokens_ref,
    state_hbm,
    norm_gain_ref,
    wr_hbm,
    wk_hbm,
    wv_hbm,
    wd_hbm,
    wl_hbm,
    wg_hbm,
    bias_ref,
    factor_ref,
    head_gain_ref,
    wm_hbm,
    gain_ref,
    routing_ref,
    score_ref,
    gate_hbm,
    up_hbm,
    down_hbm,
    out_ref,
    state,
    wr,
    wk,
    wv,
    wd,
    wl,
    wg,
    wm,
    r_rows,
    k_rows,
    v_rows,
    d_rows,
    l_rows,
    f_rows,
    g_rows,
    o_rows,
    products,
    gatherer,
    e_gate,
    e_up,
    e_down,
    own_partial,
    other_partial,
    outgoing,
    arrived,
    paired,
    crossing,
    crossed,
    results,
    returned,
    final,
    sems,
    pair_send,
    pair_recv,
    go_send,
    go_recv,
    fwd_send,
    fwd_recv,
    back_send,
    back_recv,
    local_sems,
):
    me = lax.axis_index("ep")
    side = lax.axis_index("tp")
    other = 1 - side
    seqs, heads, cells = state.shape
    rows = seqs * heads
    width = LANES // 2
    model = tokens_ref.shape[1]
    half = model // 2
    places = experts * capacity

    sources = [wk_hbm, wr_hbm, wd_hbm, wl_hbm, state_hbm, wv_hbm, wg_hbm, wm_hbm]
    targets = [wk, wr, wd, wl, state, wv, wg, wm]
    sources += [gate_hbm.at[0], up_hbm.at[0], down_hbm.at[0]]
    targets += [e_gate, e_up, e_down]
    copies = [
        pltpu.make_async_copy(a, b, sems.at[i]) for i, (a, b) in enumerate(zip(sources, targets))
    ]
    for copy in copies:
        copy.start()

    blank = jnp.zeros(arrived.shape, BF16)
    arrived[...] = blank
    paired[...] = blank
    returned[...] = blank

    barrier = pltpu.get_barrier_semaphore()
    pl.semaphore_signal(barrier, inc=1, device_id=(me, other), device_id_type=MESH)

    @pl.loop(1, experts)
    def _(k):
        pl.semaphore_signal(
            barrier, inc=1, device_id=(lax.rem(me + k, experts), side), device_id_type=MESH
        )

    normed = rms_scale(tokens_ref[...].astype(F32), norm_gain_ref[...]).astype(BF16)
    channels = heads * width
    to_head_rows(jnp.broadcast_to(factor_ref[...], (seqs, channels)), f_rows, heads)
    to_head_rows(jnp.broadcast_to(head_gain_ref[...], (seqs, channels)), g_rows, heads)
    chunk = 512
    for c in range(cells // chunk):
        at = lax.broadcasted_iota(jnp.int32, (chunk, LANES), 0) // width
        to = lax.broadcasted_iota(jnp.int32, (chunk, LANES), 1) % width
        gatherer[pl.ds(c * chunk, chunk), :] = jnp.where(
            to - at == c * (chunk // width), 1.0, 0.0
        ).astype(BF16)

    route0 = routing_ref[0:1, :]
    route1 = routing_ref[1:2, :]
    names = lax.broadcasted_iota(jnp.int32, (experts, seqs), 0)
    hot0 = jnp.where(route0 == names, 1.0, 0.0)
    hot1 = jnp.where(route1 == names, 1.0, 0.0)
    row = lax.broadcasted_iota(jnp.int32, (seqs, seqs), 0)
    column = lax.broadcasted_iota(jnp.int32, (seqs, seqs), 1)
    above = jnp.where(row < column, 1.0, 0.0).astype(BF16)
    before0 = dot(hot0.astype(BF16), above)
    before1 = dot(hot1.astype(BF16), above) + jnp.sum(hot0, axis=1, keepdims=True)
    slot0 = jnp.sum(before0 * hot0, axis=0, keepdims=True).astype(jnp.int32)
    slot1 = jnp.sum(before1 * hot1, axis=0, keepdims=True).astype(jnp.int32)
    spots = lax.broadcasted_iota(jnp.int32, (places, seqs), 0)
    place0 = jnp.where(route0 * capacity + slot0 == spots, 1.0, 0.0)
    place1 = jnp.where(route1 * capacity + slot1 == spots, 1.0, 0.0)
    placed = (place0 + place1).astype(BF16)
    place0 = place0.astype(BF16)
    place1 = place1.astype(BF16)
    difference = score_ref[0:1, :] - score_ref[1:2, :]
    difference = jnp.sum(jnp.where(row == column, difference, 0.0), axis=1, keepdims=True)
    weight0 = jax.nn.sigmoid(difference)
    weight1 = jax.nn.sigmoid(-difference)

    copies[0].wait()
    to_head_rows(dot(normed, wk[...]), k_rows, heads)
    copies[1].wait()
    to_head_rows(dot(normed, wr[...]), r_rows, heads)
    copies[2].wait()
    decay_in = dot(normed, wd[...]) + bias_ref[...]
    to_head_rows(jnp.exp(-DECAY_SCALE * jax.nn.sigmoid(decay_in)), d_rows, heads)
    copies[3].wait()
    to_head_rows(jax.nn.sigmoid(dot(normed, wl[...])), l_rows, heads)

    key = k_rows[...]
    unit = key * lax.rsqrt(jnp.sum(key * key, axis=-1, keepdims=True) * 0.5 + UNIT_EPS)
    decay = d_rows[...]
    rate = l_rows[...]
    receptance = r_rows[...]
    shifted = key * rate
    unit_rate = unit * rate
    decay_receptance = decay * receptance

    copies[4].wait()
    for c in range(cells // LANES):
        lanes = pl.ds(c * LANES, LANES)
        x = state[:, :, lanes].reshape(rows, LANES)
        products[0:rows, lanes] = (x * unit).astype(BF16)
        high, low = split(x * decay_receptance)
        products[rows : 2 * rows, lanes] = high
        products[2 * rows : 3 * rows, lanes] = low
    copies[5].wait()
    to_head_rows(dot(normed, wv[...]), v_rows, heads)
    value = v_rows[...]
    sums = dot(products[...], gatherer[...])
    removed = sums[0:rows]
    read = sums[rows : 2 * rows] + sums[2 * rows :]

    def head_sum(x):
        return jnp.sum(x, axis=-1, keepdims=True) * 0.5

    read = read - removed * head_sum(unit_rate * receptance) + value * head_sum(shifted * receptance)
    center = read - head_sum(read) * (1.0 / width)
    scaled = center * lax.rsqrt(head_sum(center * center) * (1.0 / width) + HEAD_EPS)
    own = head_sum(receptance * shifted * f_rows[...])
    o_rows[...] = scaled * g_rows[...] + own * value
    copies[6].wait()
    gating = jax.nn.sigmoid(dot(normed, wg[...]))
    merged = (from_head_rows(o_rows, seqs, heads) * gating).astype(BF16)
    copies[7].wait()
    own_partial[...] = dot(merged, wm[...]).astype(BF16)
    pl.semaphore_wait(barrier, experts)

    def to_pair(source, target, index):
        return pltpu.make_async_remote_copy(
            src_ref=source,
            dst_ref=target,
            send_sem=pair_send.at[index],
            recv_sem=pair_recv.at[index],
            device_id=(me, other),
            device_id_type=MESH,
        )

    mix_copy = to_pair(own_partial, other_partial, 0)
    mix_copy.start()
    first = lax.broadcasted_iota(jnp.int32, (rows, LANES), 1) < width
    v_high, v_low = split(value)
    m_high, m_low = split(removed)
    compact = jnp.concatenate(
        [
            jnp.where(first, v_high.astype(F32), v_low.astype(F32)).astype(BF16),
            jnp.where(first, m_high.astype(F32), m_low.astype(F32)).astype(BF16),
        ],
        axis=0,
    )

    def update_state(c):
        spread = lax.dot_general(
            compact,
            gatherer[pl.ds(c * chunk, chunk), :],
            (((1,), (1,)), ((), ())),
            preferred_element_type=F32,
        )
        for b in range(chunk // LANES):
            lanes = pl.ds(c * chunk + b * LANES, LANES)
            x = state[:, :, lanes].reshape(rows, LANES)
            v_here = spread[0:rows, b * LANES : (b + 1) * LANES]
            m_here = spread[rows:, b * LANES : (b + 1) * LANES]
            new = x * decay + v_here * shifted - m_here * unit_rate
            state[:, :, lanes] = new.reshape(seqs, heads, LANES)

    mix_copy.wait()
    mix = (own_partial[...].astype(F32) + other_partial[...].astype(F32)).astype(BF16)
    residual = tokens_ref[...].astype(F32) + mix.astype(F32)
    expert_in = rms_scale(residual, gain_ref[...])
    own_part = pl.ds(pl.multiple_of(side * half, LANES), half)
    other_part = pl.ds(pl.multiple_of(other * half, LANES), half)
    mine = jnp.where(side == 0, expert_in[:, :half], expert_in[:, half:]).astype(BF16)
    own_residual = jnp.where(side == 0, residual[:, :half], residual[:, half:])
    outgoing[...] = dot(placed, mine).reshape(experts, capacity, half).astype(BF16)
    used = pl.ds(0, sent)

    def across(source, target, send, receive, k):
        peer = lax.rem(me + k, experts)
        return pltpu.make_async_remote_copy(
            src_ref=source.at[peer, used],
            dst_ref=target.at[me, used],
            send_sem=send.at[k],
            recv_sem=receive.at[k],
            device_id=(peer, side),
            device_id_type=MESH,
        )

    def go(k):
        return across(outgoing, arrived, go_send, go_recv, k)

    def back(k):
        return across(results, returned, back_send, back_recv, k)

    def forward(k):
        source = lax.rem(me - k + experts, experts)
        return pltpu.make_async_remote_copy(
            src_ref=arrived.at[source, used],
            dst_ref=paired.at[source, used],
            send_sem=fwd_send.at[k],
            recv_sem=fwd_recv.at[k],
            device_id=(me, other),
            device_id_type=MESH,
        )

    def keep(source, target, index):
        return pltpu.make_async_copy(
            source.at[me, used], target.at[me, used], local_sems.at[index]
        )

    @pl.loop(1, experts)
    def _(j):
        go(lax.rem(j + experts // 2 - 2, experts - 1) + 1).start()

    keep(outgoing, arrived, 0).start()
    steps = cells // chunk
    for c in range(steps // 2):
        update_state(c)
    keep(outgoing, arrived, 0).wait()
    forward(0).start()

    @pl.loop(1, experts)
    def _(k):
        go(k).wait_recv()
        forward(k).start()

    x = arrived[...].astype(F32).reshape(places, half).astype(BF16)
    copies[8].wait()
    copies[9].wait()
    gate = dot(x, e_gate[own_part, :])
    up = dot(x, e_up[own_part, :])

    @pl.loop(0, experts)
    def _(k):
        forward(k).wait_recv()

    x = paired[...].astype(F32).reshape(places, half).astype(BF16)
    gate = gate + dot(x, e_gate[other_part, :])
    up = up + dot(x, e_up[other_part, :])
    hidden = (jax.nn.silu(gate) * up).astype(BF16)
    copies[10].wait()
    crossing[...] = dot(hidden, e_down[:, other_part]).astype(BF16)
    cross_copy = to_pair(crossing, crossed, 1)
    cross_copy.start()
    own_result = dot(hidden, e_down[:, own_part])
    cross_copy.wait()
    own_result = own_result + crossed[...].astype(F32)
    results[...] = own_result.reshape(experts, capacity, half).astype(BF16)

    @pl.loop(1, experts)
    def _(j):
        back(lax.rem(j + experts // 2 - 2, experts - 1) + 1).start()

    keep(results, returned, 1).start()
    for c in range(steps // 2, steps):
        update_state(c)
    keep(results, returned, 1).wait()

    @pl.loop(1, experts)
    def _(k):
        back(k).wait_recv()

    y = returned[...].astype(F32).reshape(places, half).astype(BF16)
    turned = (((0,), (0,)), ((), ()))
    total = (
        own_residual
        + weight0 * lax.dot_general(place0, y, turned, preferred_element_type=F32)
        + weight1 * lax.dot_general(place1, y, turned, preferred_element_type=F32)
    )
    final[...] = total.astype(BF16)
    final_copy = to_pair(final, out_ref.at[:, own_part], 2)
    final_copy.start()
    out_ref[:, own_part] = final[...]
    final_copy.wait()

    forward(0).wait_send()

    @pl.loop(1, experts)
    def _(k):
        go(k).wait_send()
        forward(k).wait_send()
        back(k).wait_send()


def store_kernel(layer_ref, state_ref, layer_out, state_out, sems):
    first = pltpu.make_async_copy(state_ref, state_out, sems.at[0])
    second = pltpu.make_async_copy(layer_ref, layer_out, sems.at[1])
    first.start()
    second.start()
    first.wait()
    second.wait()


def body(
    tokens,
    linear_matrix_state,
    mixer_norm_gain,
    receptance_weight,
    key_weight,
    value_weight,
    decay_weight,
    learning_rate_weight,
    output_gate_weight,
    decay_offset_bias,
    present_position_factor,
    per_head_gain,
    head_mix_weight,
    feedforward_gain,
    routing,
    router_score,
    expert_gate_weight,
    expert_up_weight,
    expert_down_weight,
):
    seqs, model = tokens.shape
    _, heads, cells = linear_matrix_state.shape
    rows = seqs * heads
    weights = (
        receptance_weight,
        key_weight,
        value_weight,
        decay_weight,
        learning_rate_weight,
        output_gate_weight,
    )
    experts = lax.axis_size("ep")
    sent = max(2, 8 * seqs * routing.shape[1] // (3 * experts))
    sent = -(-sent // 2) * 2
    capacity = -(-sent // 8) * 8
    half = model // 2
    exchange = pltpu.VMEM((experts, capacity, half), BF16)
    crosswise = pltpu.VMEM((experts * capacity, half), BF16)
    layer, state = pl.pallas_call(
        functools.partial(layer_kernel, experts, capacity, sent),
        out_shape=(
            pltpu.VMEM((seqs, model), BF16),
            pltpu.VMEM(linear_matrix_state.shape, F32),
        ),
        in_specs=[VMEM, HBM, VMEM] + [HBM] * 6 + [VMEM] * 3 + [HBM] + [VMEM] * 3 + [HBM] * 3,
        out_specs=(VMEM, VMEM),
        scratch_shapes=[pltpu.VMEM(w.shape, BF16) for w in weights]
        + [pltpu.VMEM(head_mix_weight.shape, BF16)]
        + [pltpu.VMEM((rows, LANES), F32)] * 8
        + [
            pltpu.VMEM((3 * rows, cells), BF16),
            pltpu.VMEM((cells, LANES), BF16),
            pltpu.VMEM(expert_gate_weight.shape[1:], BF16),
            pltpu.VMEM(expert_up_weight.shape[1:], BF16),
            pltpu.VMEM(expert_down_weight.shape[1:], BF16),
            pltpu.VMEM((seqs, model), BF16),
            pltpu.VMEM((seqs, model), BF16),
            exchange,
            exchange,
            exchange,
            crosswise,
            crosswise,
            exchange,
            exchange,
            pltpu.VMEM((seqs, half), BF16),
            pltpu.SemaphoreType.DMA((11,)),
            pltpu.SemaphoreType.DMA((3,)),
            pltpu.SemaphoreType.DMA((3,)),
        ]
        + [pltpu.SemaphoreType.DMA((experts,))] * 6
        + [pltpu.SemaphoreType.DMA((2,))],
        compiler_params=pltpu.CompilerParams(
            collective_id=0, has_side_effects=True, vmem_limit_bytes=61 * 2**20
        ),
        name="layer",
    )(
        tokens,
        linear_matrix_state,
        mixer_norm_gain.reshape(1, -1),
        *weights,
        decay_offset_bias.reshape(1, -1),
        present_position_factor.reshape(1, -1),
        per_head_gain.reshape(1, -1),
        head_mix_weight,
        feedforward_gain.reshape(1, -1),
        routing.T,
        router_score.T,
        expert_gate_weight,
        expert_up_weight,
        expert_down_weight,
    )
    return pl.pallas_call(
        store_kernel,
        out_shape=(
            jax.ShapeDtypeStruct((seqs, model), BF16),
            jax.ShapeDtypeStruct(linear_matrix_state.shape, F32),
        ),
        in_specs=[VMEM, VMEM],
        out_specs=(HBM, HBM),
        scratch_shapes=[pltpu.SemaphoreType.DMA((2,))],
        compiler_params=pltpu.CompilerParams(vmem_limit_bytes=4 * 2**20),
        name="store",
    )(layer, state)


def solution(mesh):
    return jax.shard_map(
        body,
        mesh=mesh,
        in_specs=(
            P("ep", None),
            P("ep", "tp", None),
            P(),
            P(None, "tp"),
            P(None, "tp"),
            P(None, "tp"),
            P(None, "tp"),
            P(None, "tp"),
            P(None, "tp"),
            P("tp"),
            P("tp"),
            P("tp"),
            P("tp", None),
            P(),
            P("ep", None),
            P("ep", None),
            P("ep", None, "tp"),
            P("ep", None, "tp"),
            P("ep", "tp", None),
        ),
        out_specs=(P("ep", None), P("ep", "tp", None)),
        check_vma=False,
    )
```

time: 40.6 us -> 29.4 us (0.72)
  Pallas kernels: 35.5 us -> 28.5 us
  local copies, waits for them, and re-layouts: 4.07 us -> 0 us
    pallas_call x2, Pallas kernels: 35.5 us -> 28.5 us  [the longest x1 27.2 us: body(): pl.pallas_call(functools.partial(layer_kernel, experts, capacity, sent),...]
    unnamed x3 -> x0, local copies, waits for them, and re-layouts: 4.07 us -> none
where the time goes in v2:
time: 29.4 us; the launch traced here: 29.2 us
  Pallas kernels  28.5 us (97%)
  between operations  0.65 us (2%)
    pallas_call x1, Pallas kernels, body(): pl.pallas_call(functools.partial(layer_kernel, experts, capacity, sent),...  27.2 us
    pallas_call x1, Pallas kernels, body(): pl.pallas_call(store_kernel, out_shape=(jax.ShapeDtypeStruct((seqs, model...  1.34 us

profile of v2, /device:TPU:0, one launch (start us, length us, event | category | flops | bytes accessed | tf_op | source)
XLA Modules:
  0.0 29.2 jit_solution(7884806210202459073)
XLA Ops:
  0.6 27.2 %layer.1 = (bf16[16,1024]{1,0:T(8,128)(2,1)S(1)}, f32[16,8,4096]{2,1,0:T(8,128)S(1)}) custom-call(bf16[16,1024]{1,0:T(8,128)(2,1)} %tokens_ref.1, f32[16,8,4096]{2,1,0:T(8,128)} %state_hbm.1, f32[1,1024]{1,0:T(1,128)} %bitcast.7, bf16[1024,512]{1,0:T(8,128)(2,1)} %wr_hbm.1, bf16[1024,512]{1,0:T(8,128)(2,1)} %wk_hbm.1, bf16[1024,512]{1,0:T(8,128)(2,1)} %wv_hbm.1, ...), custom_call_target="tpu_custom_call" | custom-call | tf_op jit(solution)/shard_map/layer/pallas_call | solution.py:445
  27.8 1.3 %store.1 = (bf16[16,1024]{1,0:T(8,128)(2,1)}, f32[16,8,4096]{2,1,0:T(8,128)}) custom-call(bf16[16,1024]{1,0:T(8,128)(2,1)S(1)} %get-tuple-element.4.layer_ref, f32[16,8,4096]{2,1,0:T(8,128)S(1)} %get-tuple-element.5.state_ref), custom_call_target="tpu_custom_call" | custom-call | tf_op jit(solution)/shard_map/store/pallas_call | solution.py:498

commit v3 on v2

--- a/solution.py
+++ b/solution.py
@@ -189,14 +189,12 @@
     weight0 = jax.nn.sigmoid(difference)
     weight1 = jax.nn.sigmoid(-difference)
 
-    copies[0].wait()
+    for copy in copies[:4]:
+        copy.wait()
     to_head_rows(dot(normed, wk[...]), k_rows, heads)
-    copies[1].wait()
     to_head_rows(dot(normed, wr[...]), r_rows, heads)
-    copies[2].wait()
     decay_in = dot(normed, wd[...]) + bias_ref[...]
     to_head_rows(jnp.exp(-DECAY_SCALE * jax.nn.sigmoid(decay_in)), d_rows, heads)
-    copies[3].wait()
     to_head_rows(jax.nn.sigmoid(dot(normed, wl[...])), l_rows, heads)
 
     key = k_rows[...]
@@ -208,7 +206,8 @@
     unit_rate = unit * rate
     decay_receptance = decay * receptance
 
-    copies[4].wait()
+    for copy in copies[4:8]:
+        copy.wait()
     for c in range(cells // LANES):
         lanes = pl.ds(c * LANES, LANES)
         x = state[:, :, lanes].reshape(rows, LANES)
@@ -216,7 +215,6 @@
         high, low = split(x * decay_receptance)
         products[rows : 2 * rows, lanes] = high
         products[2 * rows : 3 * rows, lanes] = low
-    copies[5].wait()
     to_head_rows(dot(normed, wv[...]), v_rows, heads)
     value = v_rows[...]
     sums = dot(products[...], gatherer[...])
@@ -231,10 +229,8 @@
     scaled = center * lax.rsqrt(head_sum(center * center) * (1.0 / width) + HEAD_EPS)
     own = head_sum(receptance * shifted * f_rows[...])
     o_rows[...] = scaled * g_rows[...] + own * value
-    copies[6].wait()
     gating = jax.nn.sigmoid(dot(normed, wg[...]))
     merged = (from_head_rows(o_rows, seqs, heads) * gating).astype(BF16)
-    copies[7].wait()
     own_partial[...] = dot(merged, wm[...]).astype(BF16)
     pl.semaphore_wait(barrier, experts)
 

time: 29.4 us -> 28.9 us (0.983)
  Pallas kernels: 28.5 us -> 28.1 us
    pallas_call x1, Pallas kernels: 27.2 us -> 26.7 us  [body(): pl.pallas_call(functools.partial(layer_kernel, experts, capacity, sent),...]
where the time goes in v3:
time: 28.9 us; the launch traced here: 28.7 us
  Pallas kernels  28.1 us (97%)
  between operations  0.65 us (2%)
    pallas_call x1, Pallas kernels, body(): pl.pallas_call(functools.partial(layer_kernel, experts, capacity, sent),...  26.7 us
    pallas_call x1, Pallas kernels, body(): pl.pallas_call(store_kernel, out_shape=(jax.ShapeDtypeStruct((seqs, model...  1.34 us

profile of v3, /device:TPU:0, one launch (start us, length us, event | category | flops | bytes accessed | tf_op | source)
XLA Modules:
  0.0 28.7 jit_solution(16630081785518661360)
XLA Ops:
  0.6 26.7 %layer.1 = (bf16[16,1024]{1,0:T(8,128)(2,1)S(1)}, f32[16,8,4096]{2,1,0:T(8,128)S(1)}) custom-call(bf16[16,1024]{1,0:T(8,128)(2,1)} %tokens_ref.1, f32[16,8,4096]{2,1,0:T(8,128)} %state_hbm.1, f32[1,1024]{1,0:T(1,128)} %bitcast.7, bf16[1024,512]{1,0:T(8,128)(2,1)} %wr_hbm.1, bf16[1024,512]{1,0:T(8,128)(2,1)} %wk_hbm.1, bf16[1024,512]{1,0:T(8,128)(2,1)} %wv_hbm.1, ...), custom_call_target="tpu_custom_call" | custom-call | tf_op jit(solution)/shard_map/layer/pallas_call | solution.py:441
  27.4 1.3 %store.1 = (bf16[16,1024]{1,0:T(8,128)(2,1)}, f32[16,8,4096]{2,1,0:T(8,128)}) custom-call(bf16[16,1024]{1,0:T(8,128)(2,1)S(1)} %get-tuple-element.4.layer_ref, f32[16,8,4096]{2,1,0:T(8,128)S(1)} %get-tuple-element.5.state_ref), custom_call_target="tpu_custom_call" | custom-call | tf_op jit(solution)/shard_map/store/pallas_call | solution.py:494
